TPU v7x, 32 devices: a whole 2x2x4 slice. The times are simulated.
32 devices in a mesh: fs: 4 (over z), tp: 4 (over y, x), rep: 2 (over core).
Axes of the slice: x: 2, y: 2, z: 4, core: 2. Of those that a mesh axis runs over, the one named last changes fastest.
Arguments:
- gate_grads: float32 [2, 5632, 2048], P('rep', 'fs', 'tp'), may hold values from -16 to 16, as said below
- gate_velocity: float32 [5632, 2048], P(('fs', 'rep'), 'tp'), may hold values from -31 to 31, as said below
- gate_weight: float32 [5632, 2048], P(('fs', 'rep'), 'tp'), may hold values from -4 to 4
- up_grads: float32 [2, 5632, 2048], P('rep', 'fs', 'tp'), may hold values from -16 to 16, as said below
- up_velocity: float32 [5632, 2048], P(('fs', 'rep'), 'tp'), may hold values from -31 to 31, as said below
- up_weight: float32 [5632, 2048], P(('fs', 'rep'), 'tp'), may hold values from -4 to 4
- branch_grads: float32 [2, 2048, 1024], P('rep', 'fs', 'tp'), may hold values from -16 to 16, as said below
- branch_velocity: float32 [2048, 1024], P(('fs', 'rep'), 'tp'), may hold values from -31 to 31, as said below
- branch_weight: float32 [2048, 1024], P(('fs', 'rep'), 'tp'), may hold values from -4 to 4
Outputs:
- gate_momentum: float32 [5632, 2048], P(('fs', 'rep'), 'tp')
- gate_updated: float32 [5632, 2048], P(('fs', 'rep'), 'tp')
- up_momentum: float32 [5632, 2048], P(('fs', 'rep'), 'tp')
- up_updated: float32 [5632, 2048], P(('fs', 'rep'), 'tp')
- branch_momentum: float32 [2048, 1024], P(('fs', 'rep'), 'tp')
- branch_updated: float32 [2048, 1024], P(('fs', 'rep'), 'tp')
Inputs may be any that keep to these rules, and one draw needn't show every extreme that they name: `gate_grads`: entries vary in scale over rows and over columns. `up_grads`: entries vary in scale over rows and over columns. `branch_grads`: entries vary in scale over rows and over columns. `gate_velocity`: entries vary in scale over rows and over columns. `up_velocity`: entries vary in scale over rows and over columns. `branch_velocity`: entries vary in scale over rows and over columns.
All inputs are finite; a program needn't handle non-finite values.
Results may differ from a plain program's by a relative error of at most 0.039.
Values may be sent and summed in bfloat16 or wider, within the bound.
A program may use at most 64 MiB of HBM per device.

v0:
```python
import math

import jax
import jax.numpy as jnp
from jax import lax
from jax.sharding import PartitionSpec as P

D = 2048
FF = 5632
ITERS = 3


MOMENT = 0.95
COEF_ONE = 3.4445
COEF_THREE = -4.775
COEF_FIVE = 2.0315
SAFETY = 2.0
RATE = 0.5
SHRINK = 0.95


def rounded(part):
    narrow = lax.optimization_barrier(part.astype(jnp.bfloat16))
    return narrow.astype(jnp.float32)


def gram(current):
    whole = lax.all_gather(current, "tp", axis=1, tiled=True)
    part = lax.dot_general(
        whole, current, (((0,), (0,)), ((), ())), preferred_element_type=jnp.float32
    )
    share = lax.psum_scatter(
        rounded(part).astype(jnp.bfloat16), ("fs", "rep"), scatter_dimension=0, tiled=True
    ).astype(jnp.float32)
    return (whole, share)


def spread(share):
    return lax.all_gather(share, ("fs", "rep"), axis=0, tiled=True)


def second_product(ymat, columns):
    return jnp.dot(
        lax.all_gather(ymat, "tp", axis=1, tiled=True), columns, preferred_element_type=jnp.float32
    )


def combine(current, ymat, zmat, factor):
    mixed = COEF_ONE * factor * current.astype(jnp.float32) + COEF_THREE * ymat.astype(jnp.float32)
    return (mixed + COEF_FIVE * zmat.astype(jnp.float32)).astype(jnp.bfloat16)


def orthogonalize(starts):
    firsts = [gram(current) for current in starts]
    squares = tuple((jnp.sum(jnp.square(current.astype(jnp.float32))) for current in starts))
    seconds = tuple((jnp.sum(share * share) for whole, share in firsts))
    first_sums = lax.psum(squares, ("fs", "tp", "rep"))
    gram_sums = lax.psum(seconds, ("fs", "tp", "rep"))
    finals = []
    for current, pair, first_sum, gram_sum in zip(starts, firsts, first_sums, gram_sums):
        whole, share = pair
        ratio = SAFETY * (gram_sum + 1.0) / (first_sum + 1.0)
        factor = lax.rsqrt(ratio)
        columns = spread((share / ratio).astype(jnp.bfloat16))
        ymat = (jnp.dot(whole, columns, preferred_element_type=jnp.float32) * factor).astype(
            jnp.bfloat16
        )
        zmat = second_product(ymat, columns).astype(jnp.bfloat16)
        current = combine(current, ymat, zmat, factor)
        for index in range(ITERS - 1):
            whole, share = gram(current)
            columns = spread(share.astype(jnp.bfloat16))
            ymat = jnp.dot(whole, columns, preferred_element_type=jnp.float32).astype(jnp.bfloat16)
            zmat = second_product(ymat, columns).astype(jnp.bfloat16)
            current = combine(current, ymat, zmat, 1.0)
        finals.append(current)
    return tuple(finals)


def local(
    gate_grads,
    gate_velocity,
    gate_weight,
    up_grads,
    up_velocity,
    up_weight,
    branch_grads,
    branch_velocity,
    branch_weight,
):
    totals = (
        lax.psum_scatter(
            gate_grads.astype(jnp.bfloat16), "rep", scatter_dimension=1, tiled=True
        ).astype(jnp.float32),
        lax.psum_scatter(
            up_grads.astype(jnp.bfloat16), "rep", scatter_dimension=1, tiled=True
        ).astype(jnp.float32),
        lax.psum_scatter(
            branch_grads.astype(jnp.bfloat16), "rep", scatter_dimension=1, tiled=True
        ).astype(jnp.float32),
    )
    velocities = (gate_velocity, up_velocity, branch_velocity)
    moments = [MOMENT * velocity + total[0] for velocity, total in zip(velocities, totals)]
    starts = tuple((moment.astype(jnp.bfloat16) for moment in moments))
    finals = orthogonalize(starts)
    weights = (gate_weight, up_weight, branch_weight)
    heights = (FF, FF, D)
    results = []
    for moment, weight, final, height in zip(moments, weights, finals, heights):
        results.append(moment)
        results.append(SHRINK * weight - RATE * math.sqrt(height) * final.astype(jnp.float32))
    return tuple(results)


def solution(mesh):
    placed = (
        P("rep", "fs", "tp"),
        P(("fs", "rep"), "tp"),
        P(("fs", "rep"), "tp"),
        P("rep", "fs", "tp"),
        P(("fs", "rep"), "tp"),
        P(("fs", "rep"), "tp"),
        P("rep", "fs", "tp"),
        P(("fs", "rep"), "tp"),
        P(("fs", "rep"), "tp"),
    )
    return jax.shard_map(
        local,
        mesh=mesh,
        in_specs=placed,
        out_specs=(
            P(("fs", "rep"), "tp"),
            P(("fs", "rep"), "tp"),
            P(("fs", "rep"), "tp"),
            P(("fs", "rep"), "tp"),
            P(("fs", "rep"), "tp"),
            P(("fs", "rep"), "tp"),
        ),
        check_vma=False,
    )
```

profile of v0, /device:TPU:0, one launch (start us, length us, event | category | flops | bytes accessed | tf_op | source)
XLA Modules:
  0.0 1138.2 jit_solution(9689836868072405594)
XLA Ops:
  49.5 19.3 %all_gather.99 = bf16[256,1024]{1,0:T(8,128)(2,1)S(1)} all-gather(bf16[256,256]{1,0:T(8,128)(2,1)S(1)} %get-tuple-element.13), channel_id=1, replica_groups=mesh['fs'=4,'tp'=4,'rep'=2] {'tp'}, dimensions={1}, use_global_device_ids=true | all-gather | bytes 655360 | tf_op jit(solution)/shard_map/all_gather | solution.py:28
  70.0 25.2 %all-gather.19.cloned.1.call-done = bf16[704,2048]{1,0:T(8,128)(2,1)} async-done(((bf16[704,512]{1,0:T(8,128)(2,1)}), bf16[704,2048]{1,0:T(8,128)(2,1)}) %all-gather.19.cloned.1.call-update) | async-done | bytes 2883600 | tf_op jit(solution)/shard_map/all_gather | solution.py:28
  100.3 38.7 %all-gather.37.cloned.1.call-done = bf16[704,2048]{1,0:T(8,128)(2,1)} async-done(((bf16[704,512]{1,0:T(8,128)(2,1)}), bf16[704,2048]{1,0:T(8,128)(2,1)}) %all-gather.37.cloned.1.call-update) | async-done | bytes 2883600 | tf_op jit(solution)/shard_map/all_gather | solution.py:28
  144.0 28.5 %reduce-scatter.31.cloned.1.call-done = bf16[128,256]{1,0:T(8,128)(2,1)} async-done(((bf16[1024,256]{1,0:T(8,128)(2,1)}), bf16[128,256]{1,0:T(8,128)(2,1)}) %reduce-scatter.31.cloned.1.call-update) | async-done | bytes 65552 | tf_op jit(solution)/shard_map/reduce_scatter | solution.py:32
  174.0 34.9 %reduce-scatter.15.cloned.1.call-done = bf16[256,512]{1,0:T(8,128)(2,1)} async-done(((bf16[2048,512]{1,0:T(8,128)(2,1)}), bf16[256,512]{1,0:T(8,128)(2,1)}) %reduce-scatter.15.cloned.1.call-update) | async-done | bytes 262160 | tf_op jit(solution)/shard_map/reduce_scatter | solution.py:32
  210.6 35.3 %reduce-scatter.23.cloned.1.call-done = bf16[256,512]{1,0:T(8,128)(2,1)} async-done(((bf16[2048,512]{1,0:T(8,128)(2,1)}), bf16[256,512]{1,0:T(8,128)(2,1)}) %reduce-scatter.23.cloned.1.call-update) | async-done | bytes 262160 | tf_op jit(solution)/shard_map/reduce_scatter | solution.py:32
  247.6 38.3 %all-reduce = (f32[]{:T(128)}, f32[]{:T(128)}, f32[]{:T(128)}, f32[]{:T(128)}, f32[]{:T(128)}, /*index=5*/f32[]{:T(128)}) all-reduce(f32[]{:T(128)} %fusion.26, f32[]{:T(128)} %get-tuple-element.18, f32[]{:T(128)} %fusion.28, f32[]{:T(128)} %get-tuple-element.15, ...), channel_id=1, replica_groups=mesh['fs'=4,'tp'=4,'rep'=2] {'fs','tp','rep'}, use_global_device_ids=true, to_apply=%region_3.0 | all-reduce | flops 6 | bytes 48 | tf_op jit(solution)/shard_map/psum | solution.py:58
  292.2 26.8 %all-gather.21.cloned.1.call-done = bf16[2048,512]{1,0:T(8,128)(2,1)} async-done(((bf16[256,512]{1,0:T(8,128)(2,1)}), bf16[2048,512]{1,0:T(8,128)(2,1)}) %all-gather.21.cloned.1.call-update) | async-done | bytes 2097168 | tf_op jit(solution)/shard_map/all_gather | solution.py:39
  324.0 25.5 %all-gather.39.cloned.1.call-done = bf16[2048,512]{1,0:T(8,128)(2,1)} async-done(((bf16[256,512]{1,0:T(8,128)(2,1)}), bf16[2048,512]{1,0:T(8,128)(2,1)}) %all-gather.39.cloned.1.call-update) | async-done | bytes 2097168 | tf_op jit(solution)/shard_map/all_gather | solution.py:39
  354.6 38.3 %all-gather.23.cloned.1.call-done = bf16[704,2048]{1,0:T(8,128)(2,1)} async-done(((bf16[704,512]{1,0:T(8,128)(2,1)}), bf16[704,2048]{1,0:T(8,128)(2,1)}) %all-gather.23.cloned.1.call-update) | async-done | bytes 2883600 | tf_op jit(solution)/shard_map/all_gather | solution.py:44
  398.1 38.7 %all-gather.41.cloned.1.call-done = bf16[704,2048]{1,0:T(8,128)(2,1)} async-done(((bf16[704,512]{1,0:T(8,128)(2,1)}), bf16[704,2048]{1,0:T(8,128)(2,1)}) %all-gather.41.cloned.1.call-update) | async-done | bytes 2883600 | tf_op jit(solution)/shard_map/all_gather | solution.py:44
  442.1 38.6 %all-gather.25.cloned.1.call-done = bf16[704,2048]{1,0:T(8,128)(2,1)} async-done(((bf16[704,512]{1,0:T(8,128)(2,1)}), bf16[704,2048]{1,0:T(8,128)(2,1)}) %all-gather.25.cloned.1.call-update) | async-done | bytes 2883600 | tf_op jit(solution)/shard_map/all_gather | solution.py:28
  485.8 38.7 %all-gather.43.cloned.1.call-done = bf16[704,2048]{1,0:T(8,128)(2,1)} async-done(((bf16[704,512]{1,0:T(8,128)(2,1)}), bf16[704,2048]{1,0:T(8,128)(2,1)}) %all-gather.43.cloned.1.call-update) | async-done | bytes 2883600 | tf_op jit(solution)/shard_map/all_gather | solution.py:28
  529.7 33.0 %reduce-scatter.17.cloned.1.call-done = bf16[256,512]{1,0:T(8,128)(2,1)} async-done(((bf16[2048,512]{1,0:T(8,128)(2,1)}), bf16[256,512]{1,0:T(8,128)(2,1)}) %reduce-scatter.17.cloned.1.call-update) | async-done | bytes 262160 | tf_op jit(solution)/shard_map/reduce_scatter | solution.py:32
  562.8 36.8 %reduce-scatter.25.cloned.1.call-done = bf16[256,512]{1,0:T(8,128)(2,1)} async-done(((bf16[2048,512]{1,0:T(8,128)(2,1)}), bf16[256,512]{1,0:T(8,128)(2,1)}) %reduce-scatter.25.cloned.1.call-update) | async-done | bytes 262160 | tf_op jit(solution)/shard_map/reduce_scatter | solution.py:32
  599.7 29.1 %all-gather.27.cloned.1.call-done = bf16[2048,512]{1,0:T(8,128)(2,1)} async-done(((bf16[256,512]{1,0:T(8,128)(2,1)}), bf16[2048,512]{1,0:T(8,128)(2,1)}) %all-gather.27.cloned.1.call-update) | async-done | bytes 2097168 | tf_op jit(solution)/shard_map/all_gather | solution.py:39
  633.9 25.0 %all-gather.45.cloned.1.call-done = bf16[2048,512]{1,0:T(8,128)(2,1)} async-done(((bf16[256,512]{1,0:T(8,128)(2,1)}), bf16[2048,512]{1,0:T(8,128)(2,1)}) %all-gather.45.cloned.1.call-update) | async-done | bytes 2097168 | tf_op jit(solution)/shard_map/all_gather | solution.py:39
  663.9 38.3 %all-gather.29.cloned.1.call-done = bf16[704,2048]{1,0:T(8,128)(2,1)} async-done(((bf16[704,512]{1,0:T(8,128)(2,1)}), bf16[704,2048]{1,0:T(8,128)(2,1)}) %all-gather.29.cloned.1.call-update) | async-done | bytes 2883600 | tf_op jit(solution)/shard_map/all_gather | solution.py:44
  707.4 38.7 %all-gather.47.cloned.1.call-done = bf16[704,2048]{1,0:T(8,128)(2,1)} async-done(((bf16[704,512]{1,0:T(8,128)(2,1)}), bf16[704,2048]{1,0:T(8,128)(2,1)}) %all-gather.47.cloned.1.call-update) | async-done | bytes 2883600 | tf_op jit(solution)/shard_map/all_gather | solution.py:44
  751.2 38.8 %all-gather.31.cloned.1.call-done = bf16[704,2048]{1,0:T(8,128)(2,1)} async-done(((bf16[704,512]{1,0:T(8,128)(2,1)}), bf16[704,2048]{1,0:T(8,128)(2,1)}) %all-gather.31.cloned.1.call-update) | async-done | bytes 2883600 | tf_op jit(solution)/shard_map/all_gather | solution.py:28
  795.2 38.8 %all-gather.49.cloned.1.call-done = bf16[704,2048]{1,0:T(8,128)(2,1)} async-done(((bf16[704,512]{1,0:T(8,128)(2,1)}), bf16[704,2048]{1,0:T(8,128)(2,1)}) %all-gather.49.cloned.1.call-update) | async-done | bytes 2883600 | tf_op jit(solution)/shard_map/all_gather | solution.py:28
  840.4 16.9 %all_gather.100 = bf16[1024,256]{1,0:T(8,128)(2,1)S(1)} all-gather(bf16[128,256]{1,0:T(8,128)(2,1)S(1)} %fusion.33), channel_id=1, replica_groups=mesh['fs'=4,'tp'=4,'rep'=2] {'fs','rep'}, dimensions={0}, use_global_device_ids=true | all-gather | bytes 589824 | tf_op jit(solution)/shard_map/all_gather | solution.py:39
  857.6 14.9 %all_gather.101 = bf16[256,1024]{1,0:T(8,128)(2,1)S(1)} all-gather(bf16[256,256]{1,0:T(8,128)(2,1)S(1)} %fusion.19), channel_id=1, replica_groups=mesh['fs'=4,'tp'=4,'rep'=2] {'tp'}, dimensions={1}, use_global_device_ids=true | all-gather | bytes 655360 | tf_op jit(solution)/shard_map/all_gather | solution.py:44
  885.6 25.8 %reduce-scatter.27.cloned.1.call-done = bf16[256,512]{1,0:T(8,128)(2,1)} async-done(((bf16[2048,512]{1,0:T(8,128)(2,1)}), bf16[256,512]{1,0:T(8,128)(2,1)}) %reduce-scatter.27.cloned.1.call-update) | async-done | bytes 262160 | tf_op jit(solution)/shard_map/reduce_scatter | solution.py:32
  911.4 32.8 %reduce-scatter.33.cloned.1.call-done = bf16[128,256]{1,0:T(8,128)(2,1)} async-done(((bf16[1024,256]{1,0:T(8,128)(2,1)}), bf16[128,256]{1,0:T(8,128)(2,1)}) %reduce-scatter.33.cloned.1.call-update) | async-done | bytes 65552 | tf_op jit(solution)/shard_map/reduce_scatter | solution.py:32
  944.2 16.4 %all_gather.103 = bf16[1024,256]{1,0:T(8,128)(2,1)S(1)} all-gather(bf16[128,256]{1,0:T(8,128)(2,1)} %reduce-scatter.33.cloned.1.call-done), channel_id=1, replica_groups=mesh['fs'=4,'tp'=4,'rep'=2] {'fs','rep'}, dimensions={0}, use_global_device_ids=true | all-gather | bytes 589824 | tf_op jit(solution)/shard_map/all_gather | solution.py:39
  960.9 14.4 %all_gather.104 = bf16[256,1024]{1,0:T(8,128)(2,1)S(1)} all-gather(bf16[256,256]{1,0:T(8,128)(2,1)S(1)} %convolution_convert_fusion.22), channel_id=1, replica_groups=mesh['fs'=4,'tp'=4,'rep'=2] {'tp'}, dimensions={1}, use_global_device_ids=true | all-gather | bytes 655360 | tf_op jit(solution)/shard_map/all_gather | solution.py:44
  975.7 12.1 %all_gather.105 = bf16[256,1024]{1,0:T(8,128)(2,1)S(1)} all-gather(bf16[256,256]{1,0:T(8,128)(2,1)S(1)} %fusion.21), channel_id=1, replica_groups=mesh['fs'=4,'tp'=4,'rep'=2] {'tp'}, dimensions={1}, use_global_device_ids=true | all-gather | bytes 655360 | tf_op jit(solution)/shard_map/all_gather | solution.py:28
  1009.3 28.6 %reduce-scatter.35.cloned.1.call-done = bf16[128,256]{1,0:T(8,128)(2,1)} async-done(((bf16[1024,256]{1,0:T(8,128)(2,1)}), bf16[128,256]{1,0:T(8,128)(2,1)}) %reduce-scatter.35.cloned.1.call-update) | async-done | bytes 65552 | tf_op jit(solution)/shard_map/reduce_scatter | solution.py:32
  1037.8 15.0 %all_gather.106 = bf16[1024,256]{1,0:T(8,128)(2,1)S(1)} all-gather(bf16[128,256]{1,0:T(8,128)(2,1)} %reduce-scatter.35.cloned.1.call-done), channel_id=1, replica_groups=mesh['fs'=4,'tp'=4,'rep'=2] {'fs','rep'}, dimensions={0}, use_global_device_ids=true | all-gather | bytes 589824 | tf_op jit(solution)/shard_map/all_gather | solution.py:39
  1053.2 17.2 %all_gather.107 = bf16[256,1024]{1,0:T(8,128)(2,1)S(1)} all-gather(bf16[256,256]{1,0:T(8,128)(2,1)S(1)} %convolution_convert_fusion.20), channel_id=1, replica_groups=mesh['fs'=4,'tp'=4,'rep'=2] {'tp'}, dimensions={1}, use_global_device_ids=true | all-gather | bytes 655360 | tf_op jit(solution)/shard_map/all_gather | solution.py:44
  1089.2 36.3 %all-gather.53.cloned.1.call-done = bf16[704,2048]{1,0:T(8,128)(2,1)} async-done(((bf16[704,512]{1,0:T(8,128)(2,1)}), bf16[704,2048]{1,0:T(8,128)(2,1)}) %all-gather.53.cloned.1.call-update) | async-done | bytes 2883600 | tf_op jit(solution)/shard_map/all_gather | solution.py:44
  (145 shorter events, 183.9 us)
Async XLA Ops:
  7.2 15.2 %reduce-scatter.13.cloned.1.call-start = ((), (), s32[]{:S(2)}) async-start(), calls=%async_computation.12 | async-start | bytes 2162688 | tf_op jit(solution)/shard_map/reduce_scatter | solution.py:92
  10.5 24.9 %reduce-scatter.21.cloned.1.call-start = ((), (), s32[]{:S(2)}) async-start(), calls=%async_computation.25 | async-start | bytes 2162688 | tf_op jit(solution)/shard_map/reduce_scatter | solution.py:95
  11.9 35.4 %reduce-scatter.29.cloned.1.call-start = ((), (), s32[]{:S(2)}) async-start(), calls=%async_computation.38 | async-start | bytes 393216 | tf_op jit(solution)/shard_map/reduce_scatter | solution.py:98
  12.7 82.5 %all-gather.19.cloned.1.call-start = ((), (), s32[]{:S(2)}) async-start(), calls=%async_computation.13 | async-start | bytes 3604480 | tf_op jit(solution)/shard_map/all_gather | solution.py:28
  25.9 113.1 %all-gather.37.cloned.1.call-start = ((), (), s32[]{:S(2)}) async-start(), calls=%async_computation.26 | async-start | bytes 3604480 | tf_op jit(solution)/shard_map/all_gather | solution.py:28
  38.9 133.6 %reduce-scatter.31.cloned.1.call-start = ((), (), s32[]{:S(2)}) async-start(), calls=%async_computation.39 | async-start | bytes 589824 | tf_op jit(solution)/shard_map/reduce_scatter | solution.py:32
  70.0 139.0 %reduce-scatter.15.cloned.1.call-start = ((), (), s32[]{:S(2)}) async-start(), calls=%async_computation.14 | async-start | bytes 2359296 | tf_op jit(solution)/shard_map/reduce_scatter | solution.py:32
  100.2 145.7 %reduce-scatter.23.cloned.1.call-start = ((), (), s32[]{:S(2)}) async-start(), calls=%async_computation.27 | async-start | bytes 2359296 | tf_op jit(solution)/shard_map/reduce_scatter | solution.py:32
  144.0 175.0 %all-gather.21.cloned.1.call-start = ((), (), s32[]{:S(2)}) async-start(), calls=%async_computation.15 | async-start | bytes 2359296 | tf_op jit(solution)/shard_map/all_gather | solution.py:39
  289.0 60.5 %all-gather.39.cloned.1.call-start = ((), (), s32[]{:S(2)}) async-start(), calls=%async_computation.28 | async-start | bytes 2359296 | tf_op jit(solution)/shard_map/all_gather | solution.py:39
  292.1 100.8 %all-gather.23.cloned.1.call-start = ((), (), s32[]{:S(2)}) async-start(), calls=%async_computation.16 | async-start | bytes 3604480 | tf_op jit(solution)/shard_map/all_gather | solution.py:44
  323.9 112.8 %all-gather.41.cloned.1.call-start = ((), (), s32[]{:S(2)}) async-start(), calls=%async_computation.29 | async-start | bytes 3604480 | tf_op jit(solution)/shard_map/all_gather | solution.py:44
  354.5 126.2 %all-gather.25.cloned.1.call-start = ((), (), s32[]{:S(2)}) async-start(), calls=%async_computation.17 | async-start | bytes 3604480 | tf_op jit(solution)/shard_map/all_gather | solution.py:28
  398.0 126.5 %all-gather.43.cloned.1.call-start = ((), (), s32[]{:S(2)}) async-start(), calls=%async_computation.30 | async-start | bytes 3604480 | tf_op jit(solution)/shard_map/all_gather | solution.py:28
  398.1 82.6 %copy-start.7 = (bf16[704,512]{1,0:T(8,128)(2,1)S(1)}, bf16[704,512]{1,0:T(8,128)(2,1)}, u32[]{:S(2)}) copy-start(bf16[704,512]{1,0:T(8,128)(2,1)} %fusion.3) | copy-start | bytes 2162692
  441.8 120.9 %reduce-scatter.17.cloned.1.call-start = ((), (), s32[]{:S(2)}) async-start(), calls=%async_computation.18 | async-start | bytes 2359296 | tf_op jit(solution)/shard_map/reduce_scatter | solution.py:32
  485.8 113.8 %reduce-scatter.25.cloned.1.call-start = ((), (), s32[]{:S(2)}) async-start(), calls=%async_computation.31 | async-start | bytes 2359296 | tf_op jit(solution)/shard_map/reduce_scatter | solution.py:32
  529.6 99.2 %all-gather.27.cloned.1.call-start = ((), (), s32[]{:S(2)}) async-start(), calls=%async_computation.19 | async-start | bytes 2359296 | tf_op jit(solution)/shard_map/all_gather | solution.py:39
  562.8 96.1 %all-gather.45.cloned.1.call-start = ((), (), s32[]{:S(2)}) async-start(), calls=%async_computation.32 | async-start | bytes 2359296 | tf_op jit(solution)/shard_map/all_gather | solution.py:39
  599.7 102.6 %all-gather.29.cloned.1.call-start = ((), (), s32[]{:S(2)}) async-start(), calls=%async_computation.20 | async-start | bytes 3604480 | tf_op jit(solution)/shard_map/all_gather | solution.py:44
  633.9 112.2 %all-gather.47.cloned.1.call-start = ((), (), s32[]{:S(2)}) async-start(), calls=%async_computation.33 | async-start | bytes 3604480 | tf_op jit(solution)/shard_map/all_gather | solution.py:44
  663.9 126.2 %all-gather.31.cloned.1.call-start = ((), (), s32[]{:S(2)}) async-start(), calls=%async_computation.21 | async-start | bytes 3604480 | tf_op jit(solution)/shard_map/all_gather | solution.py:28
  707.3 82.7 %copy-start.5 = (bf16[704,512]{1,0:T(8,128)(2,1)S(1)}, bf16[704,512]{1,0:T(8,128)(2,1)}, u32[]{:S(2)}) copy-start(bf16[704,512]{1,0:T(8,128)(2,1)} %add_convert_fusion.3) | copy-start | bytes 2162692
  707.4 126.7 %all-gather.49.cloned.1.call-start = ((), (), s32[]{:S(2)}) async-start(), calls=%async_computation.34 | async-start | bytes 3604480 | tf_op jit(solution)/shard_map/all_gather | solution.py:28
  751.2 133.9 %reduce-scatter.19.cloned.1.call-start = ((), (), s32[]{:S(2)}) async-start(), calls=%async_computation.22 | async-start | bytes 2359296 | tf_op jit(solution)/shard_map/reduce_scatter | solution.py:32
  795.1 116.2 %reduce-scatter.27.cloned.1.call-start = ((), (), s32[]{:S(2)}) async-start(), calls=%async_computation.35 | async-start | bytes 2359296 | tf_op jit(solution)/shard_map/reduce_scatter | solution.py:32
  839.1 105.1 %reduce-scatter.33.cloned.1.call-start = ((), (), s32[]{:S(2)}) async-start(), calls=%async_computation.40 | async-start | bytes 589824 | tf_op jit(solution)/shard_map/reduce_scatter | solution.py:32
  885.0 104.0 %all-gather.33.cloned.1.call-start = ((), (), s32[]{:S(2)}) async-start(), calls=%async_computation.23 | async-start | bytes 2359296 | tf_op jit(solution)/shard_map/all_gather | solution.py:39
  885.5 118.7 %all-gather.51.cloned.1.call-start = ((), (), s32[]{:S(2)}) async-start(), calls=%async_computation.36 | async-start | bytes 2359296 | tf_op jit(solution)/shard_map/all_gather | solution.py:39
  911.4 126.5 %reduce-scatter.35.cloned.1.call-start = ((), (), s32[]{:S(2)}) async-start(), calls=%async_computation.41 | async-start | bytes 589824 | tf_op jit(solution)/shard_map/reduce_scatter | solution.py:32
  988.9 94.4 %all-gather.35.cloned.1.call-start = ((), (), s32[]{:S(2)}) async-start(), calls=%async_computation.24 | async-start | bytes 3604480 | tf_op jit(solution)/shard_map/all_gather | solution.py:44
  994.1 131.4 %all-gather.53.cloned.1.call-start = ((), (), s32[]{:S(2)}) async-start(), calls=%async_computation.37 | async-start | bytes 3604480 | tf_op jit(solution)/shard_map/all_gather | solution.py:44
  (17 other events, 724.4 us)
Sparse Core Ops, SparseCore 0:
  10.8 11.5 reduce-scatter.12
  25.2 10.1 reduce-scatter.20
  38.2 9.0 reduce-scatter.28
  49.5 45.5 all-gather.18
  97.4 41.5 all-gather.36
  141.1 31.3 reduce-scatter.30
  174.8 34.0 reduce-scatter.14
  211.2 34.6 reduce-scatter.22
  289.1 29.7 all-gather.20
  321.0 28.5 all-gather.38
  351.9 40.9 all-gather.22
  395.2 41.5 all-gather.40
  439.1 41.5 all-gather.24
  483.0 41.5 all-gather.42
  526.7 36.0 reduce-scatter.16
  564.9 34.6 reduce-scatter.24
  601.1 27.7 all-gather.26
  630.3 28.5 all-gather.44
  661.3 40.9 all-gather.28
  704.5 41.5 all-gather.46
  748.5 41.5 all-gather.30
  792.4 41.5 all-gather.48
  836.3 38.4 reduce-scatter.18
  876.9 34.3 reduce-scatter.26
  914.2 29.9 reduce-scatter.32
  945.7 27.7 all-gather.32
  974.9 29.3 all-gather.50
  1007.1 30.6 reduce-scatter.34
  1040.2 43.0 all-gather.34
  1085.0 40.4 all-gather.52
where the time goes:
time: 1140 us
  waiting for transfers between devices  822 us (72%)
  blocking collectives  176 us (15%)
  matrix products  98.2 us (9%)
  other arithmetic  22.7 us (2%)
  between operations  18.6 us (2%)
    reduce_scatter x9, waiting for transfers between devices, gram(): lax.psum_scatter(rounded(part).astype(jnp.bfloat16), ('fs', 'rep'), scatt...  256 us
    all_gather x6, waiting for transfers between devices, gram(): whole = lax.all_gather(current, 'tp', axis=1, tiled=True)  219 us
    all_gather x6, waiting for transfers between devices, second_product(): lax.all_gather(ymat, 'tp', axis=1, tiled=True)  202 us
    all_gather x6, waiting for transfers between devices, spread(): return lax.all_gather(share, ('fs', 'rep'), axis=0, tiled=True)  117 us
    all_gather x3, blocking collectives, spread(): return lax.all_gather(share, ('fs', 'rep'), axis=0, tiled=True)  48.3 us
    all_gather x3, blocking collectives, second_product(): lax.all_gather(ymat, 'tp', axis=1, tiled=True)  46.5 us
    all_gather x3, blocking collectives, gram(): whole = lax.all_gather(current, 'tp', axis=1, tiled=True)  42.4 us
    psum x1, blocking collectives, orthogonalize(): gram_sums = lax.psum(seconds, ('fs', 'tp', 'rep'))  38.3 us
  transfers between devices with their start and end apart: 30, of which 28 were waited for; matrix products, arithmetic and copies ran while one was open for 10% of the time, Pallas kernels for 0%

commit v1 on v0

v1 whole, which is shorter than its diff:
```python
import functools
import math

import jax
import jax.numpy as jnp
from jax import lax
from jax.experimental import pallas as pl
from jax.experimental.pallas import tpu as pltpu
from jax.sharding import PartitionSpec as P

MOMENT = 0.95
COEF_ONE = 3.4445
COEF_THREE = -4.775
COEF_FIVE = 2.0315
SAFETY = 2.0
RATE = 0.5
SHRINK = 0.95
ITERS = 3
TILE = 512


def polynomial_kernel(size, tile, scale_ref, g_ref, q_ref, s0, s1, s2, s3):
    count = size // tile
    pairs = count * (count + 1) // 2

    def product(left, right, out, finish):
        def step(t, carry):
            i = lax.rem(t, count)
            j = lax.rem(i + t // count, count)
            rows = pl.ds(pl.multiple_of(i * tile, tile), tile)
            cols = pl.ds(pl.multiple_of(j * tile, tile), tile)
            acc = jnp.dot(left[rows, :], right[:, cols], preferred_element_type=jnp.float32)
            value = finish(acc, rows, cols, i == j).astype(jnp.bfloat16)
            out[rows, cols] = value

            @pl.when(i != j)
            def _():
                out[cols, rows] = value.T

            return carry

        lax.fori_loop(0, pairs, step, 0)

    def plain(acc, rows, cols, diagonal):
        return acc

    def scaled(acc, rows, cols, diagonal):
        return acc * scale_ref[0, 0]

    def quadratic(gram):
        def finish(acc, rows, cols, diagonal):
            here = lax.broadcasted_iota(jnp.int32, (tile, tile), 0)
            there = lax.broadcasted_iota(jnp.int32, (tile, tile), 1)
            unit = jnp.where(diagonal, COEF_ONE, 0.0)
            eye = jnp.where(here == there, unit, 0.0)
            return eye + COEF_THREE * gram[rows, cols].astype(jnp.float32) + COEF_FIVE * acc

        return finish

    product(g_ref, g_ref, s0, quadratic(g_ref))
    product(g_ref, s0, s1, plain)
    product(s1, s0, s2, plain)
    product(s2, s2, s1, quadratic(s2))
    product(s0, s1, s3, plain)
    product(s2, s1, s0, plain)
    product(s0, s1, q_ref, plain)
    product(q_ref, q_ref, s0, quadratic(q_ref))
    product(s3, s0, q_ref, scaled)


def polynomial(gram, scale):
    size = gram.shape[0]
    tile = min(TILE, size)
    matrix = pltpu.VMEM((size, size), jnp.bfloat16)
    return pl.pallas_call(
        functools.partial(polynomial_kernel, size, tile),
        out_shape=jax.ShapeDtypeStruct((size, size), jnp.bfloat16),
        in_specs=[
            pl.BlockSpec(memory_space=pltpu.SMEM),
            pl.BlockSpec(memory_space=pltpu.VMEM),
        ],
        out_specs=pl.BlockSpec(memory_space=pltpu.VMEM),
        scratch_shapes=[matrix] * 4,
        compiler_params=pltpu.CompilerParams(
            vmem_limit_bytes=min(64000 * 1024, 6 * 2 * size * size + 12 * 1024 * 1024)
        ),
        cost_estimate=pl.CostEstimate(
            flops=12 * size**3, bytes_accessed=4 * size * size, transcendentals=0
        ),
        name=f"polynomial_{size}",
    )(scale.reshape(1, 1), gram)


def normalized(raw):
    wide = raw.astype(jnp.float32)
    size = raw.shape[0]
    here = lax.broadcasted_iota(jnp.int32, (size, size), 0)
    there = lax.broadcasted_iota(jnp.int32, (size, size), 1)
    first = jnp.sum(jnp.where(here == there, wide, 0.0))
    second = jnp.sum(wide * wide)
    ratio = SAFETY * (second + 1.0) / (first + 1.0)
    return (wide / ratio).astype(jnp.bfloat16), lax.rsqrt(ratio)


def partial_gram(whole, current):
    return lax.dot_general(
        whole, current, (((0,), (0,)), ((), ())), preferred_element_type=jnp.float32
    ).astype(jnp.bfloat16)


def assemble(blocks, down, across):
    _, height, width = blocks.shape
    grid = blocks.reshape(down, across, height, width).transpose(0, 2, 1, 3)
    return grid.reshape(down * height, across * width)


def local(nfs, ntp, nrep, *args):
    grads, velocities, weights = args[0::3], args[1::3], args[2::3]
    totals = [
        lax.psum_scatter(g.astype(jnp.bfloat16), "rep", scatter_dimension=1, tiled=True)[0]
        for g in grads
    ]
    moments = [MOMENT * v + t.astype(jnp.float32) for v, t in zip(velocities, totals)]
    starts = [moment.astype(jnp.bfloat16) for moment in moments]
    wholes = [lax.all_gather(start, "tp", axis=1, tiled=True) for start in starts]
    parts = [partial_gram(whole, start) for whole, start in zip(wholes, starts)]

    size, width = parts[0].shape
    pair = jnp.stack([part.reshape(nfs, size // nfs, width) for part in parts[:nrep]], axis=1)
    share = lax.psum_scatter(
        pair.reshape(nrep * size, width), ("fs", "rep"), scatter_dimension=0, tiled=True
    )
    blocks = lax.all_gather(share, ("fs", "tp"), axis=0, tiled=False)
    gram, scale = normalized(assemble(blocks, nfs, ntp))
    large = polynomial(gram, scale)
    column = lax.axis_index("tp") * width
    mine = lax.dynamic_slice(large, (0, column), (size, width))
    columns = lax.all_gather(mine, "rep", axis=0, tiled=False)

    last = lax.psum_scatter(parts[nrep], ("fs", "rep"), scatter_dimension=0, tiled=True)
    blocks = lax.all_gather(last, ("fs", "rep", "tp"), axis=0, tiled=False)
    gram, scale = normalized(assemble(blocks, nfs * nrep, ntp))
    small = polynomial(gram, scale)
    height, width = parts[nrep].shape
    column = lax.axis_index("tp") * width
    factors = [columns[index] for index in range(nrep)]
    factors.append(lax.dynamic_slice(small, (0, column), (height, width)))

    results = []
    for moment, weight, whole, factor in zip(moments, weights, wholes, factors):
        rows = moment.shape[0] * nfs * nrep
        final = jnp.dot(whole, factor, preferred_element_type=jnp.float32)
        results.append(moment)
        results.append(SHRINK * weight - RATE * math.sqrt(rows) * final)
    return tuple(results)


def solution(mesh):
    sizes = mesh.shape
    split = P(("fs", "rep"), "tp")
    return jax.shard_map(
        functools.partial(local, sizes["fs"], sizes["tp"], sizes["rep"]),
        mesh=mesh,
        in_specs=(P("rep", "fs", "tp"), split, split) * 3,
        out_specs=(split,) * 6,
        check_vma=False,
    )
```

time: 1140 us -> 570 us (0.50)
  waiting for transfers between devices: 822 us -> 287 us
  blocking collectives: 176 us -> 14.7 us
  Pallas kernels: 0 us -> 155 us
  matrix products: 98.2 us -> 18 us
  local copies, waits for them, and re-layouts: 0.1 us -> 28.4 us
  other arithmetic: 22.7 us -> 48.8 us
    all_gather x18 -> x5, waiting for transfers between devices: 538 us -> 195 us  [the longest x1 113 us: local(): blocks = lax.all_gather(share, ('fs', 'tp'), axis=0, tiled=False)]
    reduce_scatter x12 -> x5, waiting for transfers between devices: 283 us -> 92 us  [the longest x1 34.9 us: local(): lax.psum_scatter(pair.reshape(nrep * size, width), ('fs', 'rep'), scatter...]
    pallas_call x0 -> x2, Pallas kernels: none -> 155 us  [polynomial(): pl.pallas_call(functools.partial(polynomial_kernel, size, tile), out_shap...]
    all_gather x9 -> x1, blocking collectives: 137 us -> 14.7 us  [local(): lax.all_gather(start, 'tp', axis=1, tiled=True)]
    dot_general x27 -> x6, matrix products: 98.2 us -> 18 us  [the longest x3 9.59 us: local(): final = jnp.dot(whole, factor, preferred_element_type=jnp.float32)]
    psum x1 -> x0, blocking collectives: 38.3 us -> none  [orthogonalize(): gram_sums = lax.psum(seconds, ('fs', 'tp', 'rep'))]
    convert_element_type x6 -> x8, other arithmetic: 8.68 us -> 26.2 us  [the longest x2 13.4 us: normalized(): wide = raw.astype(jnp.float32)]
    convert_element_type x0 -> x1, local copies, waits for them, and re-layouts: none -> 12.2 us  [normalized(): return ((wide / ratio).astype(jnp.bfloat16), lax.rsqrt(ratio))]
  transfers between devices with their start and end apart: 30 -> 10, of which waited for: 28 -> 8; matrix products, arithmetic and copies ran while one was open for 10% -> 15% of each run, Pallas kernels for 0% -> 27%
where the time goes in v1:
time: 570 us; the launch traced here: 569 us
  waiting for transfers between devices  287 us (50%)
  Pallas kernels  155 us (27%)
  other arithmetic  48.8 us (9%)
  local copies, waits for them, and re-layouts  28.4 us (5%)
  matrix products  18 us (3%)
  between operations  17.1 us (3%)
  blocking collectives  14.7 us (3%)
    pallas_call x2, Pallas kernels, polynomial(): pl.pallas_call(functools.partial(polynomial_kernel, size, tile), out_shap...  155 us
    all_gather x1, waiting for transfers between devices, local(): blocks = lax.all_gather(share, ('fs', 'tp'), axis=0, tiled=False)  113 us
    all_gather x2, waiting for transfers between devices, local(): lax.all_gather(start, 'tp', axis=1, tiled=True)  81.8 us
    reduce_scatter x1, waiting for transfers between devices, local(): lax.psum_scatter(pair.reshape(nrep * size, width), ('fs', 'rep'), scatter...  34.9 us
    reduce_scatter x1, waiting for transfers between devices, local(): lax.psum_scatter(parts[nrep], ('fs', 'rep'), scatter_dimension=0, tiled=T...  32.5 us
    reduce_scatter x3, waiting for transfers between devices, local(): lax.psum_scatter(g.astype(jnp.bfloat16), 'rep', scatter_dimension=1, tile...  24.6 us
    all_gather x1, blocking collectives, local(): lax.all_gather(start, 'tp', axis=1, tiled=True)  14.7 us
    convert_element_type x2, other arithmetic, normalized(): wide = raw.astype(jnp.float32)  13.4 us
  transfers between devices with their start and end apart: 10, of which 8 were waited for; matrix products, arithmetic and copies ran while one was open for 15% of the time, Pallas kernels for 27%

profile of v1, /device:TPU:0, one launch (start us, length us, event | category | flops | bytes accessed | tf_op | source)
XLA Modules:
  0.0 569.3 jit_solution(16473423588560320151)
XLA Ops:
  7.2 3.2 convert_element_type.92
  10.6 1.3 convert_element_type.87
  11.9 10.5 %reduce-scatter.8.cloned.1.call-done = bf16[1,704,512]{2,1,0:T(8,128)(2,1)} async-done(((bf16[1,1408,512]{2,1,0:T(8,128)(2,1)}), bf16[1,704,512]{2,1,0:T(8,128)(2,1)}) %reduce-scatter.8.cloned.1.call-update) | async-done | bytes 720912 | tf_op jit(solution)/shard_map/reduce_scatter | solution.py:120
  22.4 3.2 fusion.18
  25.7 9.7 %reduce-scatter.6.cloned.1.call-done = bf16[1,704,512]{2,1,0:T(8,128)(2,1)} async-done(((bf16[1,1408,512]{2,1,0:T(8,128)(2,1)}), bf16[1,704,512]{2,1,0:T(8,128)(2,1)}) %reduce-scatter.6.cloned.1.call-update) | async-done | bytes 720912 | tf_op jit(solution)/shard_map/reduce_scatter | solution.py:120
  35.4 2.7 fusion.19
  39.0 41.7 %all-gather.11.cloned.1.call-done = bf16[704,2048]{1,0:T(8,128)(2,1)} async-done(((bf16[704,512]{1,0:T(8,128)(2,1)}), bf16[704,2048]{1,0:T(8,128)(2,1)}) %all-gather.11.cloned.1.call-update) | async-done | bytes 2883600 | tf_op jit(solution)/shard_map/all_gather | solution.py:125
  80.7 3.7 convolution_convert_fusion
  84.4 40.2 %all-gather.9.cloned.1.call-done = bf16[704,2048]{1,0:T(8,128)(2,1)} async-done(((bf16[704,512]{1,0:T(8,128)(2,1)}), bf16[704,2048]{1,0:T(8,128)(2,1)}) %all-gather.9.cloned.1.call-update) | async-done | bytes 2883600 | tf_op jit(solution)/shard_map/all_gather | solution.py:125
  124.5 3.7 convolution_convert_fusion.1
  128.2 2.3 pad_maximum_fusion
  130.6 4.4 reduce-scatter.12.cloned.1.call-done
  134.9 1.6 fusion.17
  136.6 14.7 %all_gather.33 = bf16[256,1024]{1,0:T(8,128)(2,1)S(1)} all-gather(bf16[256,256]{1,0:T(8,128)(2,1)S(1)} %get-tuple-element.10), channel_id=1, replica_groups=mesh['fs'=4,'tp'=4,'rep'=2] {'tp'}, dimensions={1}, use_global_device_ids=true | all-gather | bytes 655360 | tf_op jit(solution)/shard_map/all_gather | solution.py:125
  152.0 1.1 convolution_convert_fusion.2
  153.3 34.9 %reduce-scatter.10.cloned.1.call-done = bf16[512,512]{1,0:T(8,128)(2,1)} async-done(((bf16[4096,512]{1,0:T(8,128)(2,1)}), bf16[512,512]{1,0:T(8,128)(2,1)}) %reduce-scatter.10.cloned.1.call-update) | async-done | bytes 524304 | tf_op jit(solution)/shard_map/reduce_scatter | solution.py:130
  188.2 32.5 %reduce-scatter.14.cloned.1.call-done = bf16[128,256]{1,0:T(8,128)(2,1)} async-done(((bf16[1024,256]{1,0:T(8,128)(2,1)}), bf16[128,256]{1,0:T(8,128)(2,1)}) %reduce-scatter.14.cloned.1.call-update) | async-done | bytes 65552 | tf_op jit(solution)/shard_map/reduce_scatter | solution.py:140
  220.8 113.3 %all-gather.13.cloned.1.call-done = bf16[8192,512]{1,0:T(8,128)(2,1)} async-done(((bf16[512,512]{1,0:T(8,128)(2,1)}), bf16[8192,512]{1,0:T(8,128)(2,1)}) %all-gather.13.cloned.1.call-update) | async-done | bytes 8388624 | tf_op jit(solution)/shard_map/all_gather | solution.py:133
  334.1 11.5 %convert_element_type.123 = f32[8192,512]{1,0:T(8,128)} convert(bf16[8192,512]{1,0:T(8,128)(2,1)} %all-gather.13.cloned.1.call-done) | non-fusion elementwise | flops 4194304 | bytes 25165824 | tf_op jit(solution)/shard_map/convert_element_type | solution.py:95
  345.7 9.6 %select_reduce_fusion = (f32[]{:T(128)}, f32[]{:T(128)}) fusion(f32[4,512,4,512]{3,1,2,0:T(8,128)} %bitcast.48, s32[4,512]{1,0:T(4,128)S(1)} %multiply_add_fusion), kind=kLoop, calls=%fused_computation.1 | loop fusion | flops 20971518 | bytes 16785416 | tf_op jit(solution)/shard_map/reduce_sum | solution.py:99
  356.6 8.3 %divide_convert_fusion = bf16[8192,512]{1,0:T(8,128)(2,1)} fusion(f32[]{:T(128)S(6)} %div.28, bf16[8192,512]{1,0:T(8,128)(2,1)} %all-gather.13.cloned.1.call-done), kind=kLoop, calls=%fused_computation | loop fusion | flops 12582912 | bytes 16777220 | tf_op jit(solution)/shard_map/convert.8
  364.9 12.2 %copy.18 = bf16[4,512,4,512]{3,2,1,0:T(4,128)(2,1)} copy(bf16[4,512,4,512]{3,1,2,0:T(8,128)(2,1)} %bitcast.49) | data formatting | bytes 16777216 | tf_op jit(solution)/shard_map/convert_element_type | solution.py:102
  377.1 10.2 %copy.20 = bf16[256,8,4,512]{3,1,2,0:T(8,128)(2,1)} copy(bf16[256,8,4,512]{3,2,1,0:T(4,128)(2,1)} %bitcast.50) | data formatting | bytes 16777216
  387.3 132.6 %polynomial_2048.1 = bf16[2048,2048]{1,0:T(8,128)(2,1)} custom-call(f32[1,1]{1,0:T(1,128)} %bitcast.10.scale_ref, bf16[2048,2048]{1,0:T(8,128)(2,1)} %bitcast.53), custom_call_target="tpu_custom_call" | custom-call | flops 103079215104 | bytes 16777216 | tf_op jit(solution)/shard_map/polynomial_2048/pallas_call | solution.py:75
  520.0 3.1 constant_dynamic-slice_fusion
  523.1 1.9 convert_element_type.124
  525.0 1.9 select_reduce_fusion.1
  528.8 1.6 copy.19
  530.9 21.9 %polynomial_1024.1 = bf16[1024,1024]{1,0:T(8,128)(2,1)S(1)} custom-call(f32[1,1]{1,0:T(1,128)} %bitcast.17.scale_ref, bf16[1024,1024]{1,0:T(8,128)(2,1)S(1)} %bitcast.47), custom_call_target="tpu_custom_call" | custom-call | flops 12884901888 | bytes 4194304 | tf_op jit(solution)/shard_map/polynomial_1024/pallas_call | solution.py:75
  552.8 1.0 fusion.14
  553.9 5.8 %multiply_subtract_fusion.1 = f32[704,512]{1,0:T(8,128)} fusion(f32[704,512]{1,0:T(8,128)} %param.11, bf16[704,2048]{1,0:T(8,128)(2,1)} %all-gather.9.cloned.1.call-done, bf16[4096,512]{1,0:T(8,128)(2,1)} %all-gather.15.cloned.1.call-done), kind=kOutput, calls=%fused_computation.18 | convolution fusion | flops 1477476352 | bytes 7864320 | tf_op jit(solution)/shard_map/dot_general | solution.py:152
  559.7 2.8 multiply_subtract_fusion
  (54 shorter events, 3.1 us)
Async XLA Ops:
  7.2 3.4 copy-start.3
  7.2 15.2 %reduce-scatter.8.cloned.1.call-start = ((), (), s32[]{:S(2)}) async-start(), calls=%async_computation.7 | async-start | bytes 2162688 | tf_op jit(solution)/shard_map/reduce_scatter | solution.py:120
  10.5 24.9 %reduce-scatter.6.cloned.1.call-start = ((), (), s32[]{:S(2)}) async-start(), calls=%async_computation.5 | async-start | bytes 2162688 | tf_op jit(solution)/shard_map/reduce_scatter | solution.py:120
  11.9 23.6 %copy-start.6 = (f32[704,512]{1,0:T(8,128)S(1)}, f32[704,512]{1,0:T(8,128)}, u32[]{:S(2)}) copy-start(f32[704,512]{1,0:T(8,128)} %param.10) | copy-start | bytes 4325380
  11.9 68.8 %all-gather.11.cloned.1.call-start = ((), (), s32[]{:S(2)}) async-start(), calls=%async_computation.8 | async-start | bytes 3604480 | tf_op jit(solution)/shard_map/all_gather | solution.py:125
  25.6 12.6 %copy-start.7 = (f32[1,512,256]{2,1,0:T(8,128)S(1)}, f32[1,512,256]{2,1,0:T(8,128)}, u32[]{:S(2)}) copy-start(f32[1,512,256]{2,1,0:T(8,128)} %param.15) | copy-start | bytes 1572868
  25.6 55.1 %copy-start.4 = (bf16[704,512]{1,0:T(8,128)(2,1)S(1)}, bf16[704,512]{1,0:T(8,128)(2,1)}, u32[]{:S(2)}) copy-start(bf16[704,512]{1,0:T(8,128)(2,1)} %get-tuple-element.12) | copy-start | bytes 2162692
  25.6 98.9 %all-gather.9.cloned.1.call-start = ((), (), s32[]{:S(2)}) async-start(), calls=%async_computation.6 | async-start | bytes 3604480 | tf_op jit(solution)/shard_map/all_gather | solution.py:125
  38.1 96.8 %reduce-scatter.12.cloned.1.call-start = ((), (), s32[]{:S(2)}) async-start(), calls=%async_computation.10 | async-start | bytes 393216 | tf_op jit(solution)/shard_map/reduce_scatter | solution.py:120
  39.0 85.6 %copy-start.5 = (bf16[704,512]{1,0:T(8,128)(2,1)S(1)}, bf16[704,512]{1,0:T(8,128)(2,1)}, u32[]{:S(2)}) copy-start(bf16[704,512]{1,0:T(8,128)(2,1)} %get-tuple-element.14) | copy-start | bytes 2162692
  39.0 149.2 %reduce-scatter.10.cloned.1.call-start = ((), (), s32[]{:S(2)}) async-start(), calls=%async_computation.9 | async-start | bytes 4718592 | tf_op jit(solution)/shard_map/reduce_scatter | solution.py:130
  130.5 4.4 copy-start.8
  130.5 90.2 %reduce-scatter.14.cloned.1.call-start = ((), (), s32[]{:S(2)}) async-start(), calls=%async_computation.11 | async-start | bytes 589824 | tf_op jit(solution)/shard_map/reduce_scatter | solution.py:140
  151.3 0.8 copy-start.1
  153.2 180.9 %all-gather.13.cloned.1.call-start = ((), (), s32[]{:S(2)}) async-start(), calls=%async_computation.12 | async-start | bytes 8912896 | tf_op jit(solution)/shard_map/all_gather | solution.py:133
  188.2 334.9 %all-gather.17.cloned.1.call-start = ((), (), s32[]{:S(2)}) async-start(), calls=%async_computation.14 | async-start | bytes 2162688 | tf_op jit(solution)/shard_map/all_gather | solution.py:141
  220.8 333.1 %all-gather.15.cloned.1.call-start = ((), (), s32[]{:S(2)}) async-start(), calls=%async_computation.13 | async-start | bytes 6291456 | tf_op jit(solution)/shard_map/all_gather | solution.py:138
  525.0 3.3 copy-start
  530.9 21.9 %copy-start.2 = (bf16[256,1024]{1,0:T(8,128)(2,1)S(1)}, bf16[256,1024]{1,0:T(8,128)(2,1)}, u32[]{:S(2)}) copy-start(bf16[256,1024]{1,0:T(8,128)(2,1)} %copy-done.1) | copy-start | bytes 1572868
  530.9 21.9 %copy-start.9 = (f32[256,256]{1,0:T(8,128)S(1)}, f32[256,256]{1,0:T(8,128)}, u32[]{:S(2)}) copy-start(f32[256,256]{1,0:T(8,128)} %param.17) | copy-start | bytes 786436
  553.9 5.8 %copy-start.11 = (bf16[704,2048]{1,0:T(8,128)(2,1)S(1)}, bf16[704,2048]{1,0:T(8,128)(2,1)}, u32[]{:S(2)}) copy-start(bf16[704,2048]{1,0:T(8,128)(2,1)} %all-gather.11.cloned.1.call-done) | copy-start | bytes 8650756
  553.9 5.8 %copy-start.10 = (bf16[4096,512]{1,0:T(8,128)(2,1)S(1)}, bf16[4096,512]{1,0:T(8,128)(2,1)}, u32[]{:S(2)}) copy-start(bf16[4096,512]{1,0:T(8,128)(2,1)} %all-gather.15.cloned.1.call-done) | copy-start | bytes 12582916
  553.9 5.8 %copy-start.12 = (f32[704,512]{1,0:T(8,128)S(1)}, f32[704,512]{1,0:T(8,128)}, u32[]{:S(2)}) copy-start(f32[704,512]{1,0:T(8,128)} %param.14) | copy-start | bytes 4325380
Sparse Core Ops, SparseCore 0:
  10.8 11.5 reduce-scatter.7
  25.2 10.1 reduce-scatter.5
  37.8 42.8 all-gather.10
  82.9 41.5 all-gather.8
  127.2 7.7 reduce-scatter.11
  137.1 51.0 reduce-scatter.9
  191.0 29.7 reduce-scatter.13
  223.5 110.5 all-gather.12
  337.0 54.3 all-gather.16
  523.2 12.2 all-gather.14

commit v2 on v1

v2 whole, which is shorter than its diff:
```python
import functools
import math

import jax
import jax.numpy as jnp
from jax import lax
from jax.experimental import pallas as pl
from jax.experimental.pallas import tpu as pltpu
from jax.sharding import PartitionSpec as P

MOMENT = 0.95
COEF_ONE = 3.4445
COEF_THREE = -4.775
COEF_FIVE = 2.0315
SAFETY = 2.0
RATE = 0.5
SHRINK = 0.95
ITERS = 3
TILE = 512


def polynomial_kernel(across, tile, column_ref, raw_ref, q_ref, g, s0, s1, s2, s3, c0, c1):
    blocks, height, breadth = raw_ref.shape
    size, width = q_ref.shape
    count = size // tile
    pairs = count * (count + 1) // 2
    here = lax.broadcasted_iota(jnp.int32, (height, breadth), 0)
    there = lax.broadcasted_iota(jnp.int32, (height, breadth), 1)

    def sums(t, carry):
        first, second = carry
        wide = raw_ref[t].astype(jnp.float32)
        shift = lax.rem(t, across) * breadth - t // across * height
        trace = jnp.where(here == there + shift, wide, 0.0)
        return (
            first + jnp.sum(trace, axis=0, keepdims=True),
            second + jnp.sum(wide * wide, axis=0, keepdims=True),
        )

    zero = jnp.zeros((1, breadth), jnp.float32)
    first, second = lax.fori_loop(0, blocks, sums, (zero, zero))
    first = jnp.sum(first, axis=1, keepdims=True)
    second = jnp.sum(second, axis=1, keepdims=True)
    ratio = SAFETY * (second + 1.0) / (first + 1.0)
    inverse, scale = 1.0 / ratio, lax.rsqrt(ratio)

    def normalize(t, carry):
        rows = pl.ds(pl.multiple_of(t // across * height, height), height)
        cols = pl.ds(pl.multiple_of(lax.rem(t, across) * breadth, breadth), breadth)
        g[rows, cols] = (raw_ref[t].astype(jnp.float32) * inverse).astype(jnp.bfloat16)
        return carry

    lax.fori_loop(0, blocks, normalize, 0)

    def quadratic(acc, gram, shift):
        down = lax.broadcasted_iota(jnp.int32, acc.shape, 0)
        over = lax.broadcasted_iota(jnp.int32, acc.shape, 1)
        eye = jnp.where(down == over + shift, COEF_ONE, 0.0)
        return eye + COEF_THREE * gram.astype(jnp.float32) + COEF_FIVE * acc

    def product(left, right, out, poly):
        def step(t, carry):
            i = lax.rem(t, count)
            j = lax.rem(i + t // count, count)
            rows = pl.ds(pl.multiple_of(i * tile, tile), tile)
            cols = pl.ds(pl.multiple_of(j * tile, tile), tile)
            acc = jnp.dot(left[rows, :], right[:, cols], preferred_element_type=jnp.float32)
            if poly:
                acc = quadratic(acc, left[rows, cols], (j - i) * tile)
            value = acc.astype(jnp.bfloat16)
            out[rows, cols] = value

            @pl.when(i != j)
            def _():
                out[cols, rows] = value.T

            return carry

        lax.fori_loop(0, pairs, step, 0)

    column = pl.multiple_of(column_ref[0, 0] * width, width)
    mine = pl.ds(column, width)

    def panel(left, right, out, kind):
        def step(i, carry):
            rows = pl.ds(pl.multiple_of(i * tile, tile), tile)
            acc = jnp.dot(left[rows, :], right[...], preferred_element_type=jnp.float32)
            if kind == "poly":
                acc = quadratic(acc, left[rows, mine], column - i * tile)
            if kind == "scale":
                acc = acc * scale
            out[rows, :] = acc.astype(jnp.bfloat16)
            return carry

        lax.fori_loop(0, count, step, 0)

    product(g, g, s0, True)
    product(g, s0, s1, False)
    product(s1, s0, s2, False)
    product(s2, s2, s1, True)
    product(s2, s1, s3, False)
    product(s3, s1, g, False)
    c1[...] = g[:, mine]
    panel(g, c1, c0, "poly")
    panel(s1, c0, c1, "")
    panel(s0, c1, q_ref, "scale")


def polynomial(blocks, across):
    size = blocks.shape[2] * across
    width = blocks.shape[2]
    tile = min(TILE, size)
    matrix = pltpu.VMEM((size, size), jnp.bfloat16)
    strip = pltpu.VMEM((size, width), jnp.bfloat16)
    return pl.pallas_call(
        functools.partial(polynomial_kernel, across, tile),
        out_shape=jax.ShapeDtypeStruct((size, width), jnp.bfloat16),
        in_specs=[
            pl.BlockSpec(memory_space=pltpu.SMEM),
            pl.BlockSpec(memory_space=pltpu.VMEM),
        ],
        out_specs=pl.BlockSpec(memory_space=pltpu.VMEM),
        scratch_shapes=[matrix] * 5 + [strip] * 2,
        compiler_params=pltpu.CompilerParams(
            vmem_limit_bytes=12 * size * size + 6 * size * width + 8 * 1024 * 1024
        ),
        cost_estimate=pl.CostEstimate(
            flops=10 * size**3, bytes_accessed=3 * size * size, transcendentals=0
        ),
        name=f"polynomial_{size}",
    )(lax.axis_index("tp").astype(jnp.int32).reshape(1, 1), blocks)


def partial_gram(whole, current):
    return lax.dot_general(
        whole, current, (((0,), (0,)), ((), ())), preferred_element_type=jnp.float32
    ).astype(jnp.bfloat16)


def local(nfs, ntp, nrep, *args):
    grads, velocities, weights = args[0::3], args[1::3], args[2::3]
    totals = [
        lax.psum_scatter(g.astype(jnp.bfloat16), "rep", scatter_dimension=1, tiled=True)[0]
        for g in grads
    ]
    moments = [MOMENT * v + t.astype(jnp.float32) for v, t in zip(velocities, totals)]
    starts = [moment.astype(jnp.bfloat16) for moment in moments]
    starts = lax.optimization_barrier(starts)
    wholes = [lax.all_gather(start, "tp", axis=1, tiled=True) for start in starts]
    parts = [partial_gram(whole, start) for whole, start in zip(wholes, starts)]

    shares = nfs * nrep
    size, width = parts[0].shape
    depth, narrow = parts[nrep].shape
    fold = width // narrow
    pair = jnp.stack([part.reshape(nfs, size // nfs, width) for part in parts[:nrep]], axis=1)
    pair = pair.reshape(shares, size // nfs, width)
    third = parts[nrep].reshape(shares, fold, depth // shares // fold, narrow)
    third = jnp.concatenate([third[:, index] for index in range(fold)], axis=2)
    both = jnp.concatenate([pair, third], axis=1)
    share = lax.psum_scatter(
        both.reshape(-1, width), ("fs", "rep"), scatter_dimension=0, tiled=True
    )
    blocks = lax.all_gather(share[: size // nfs], ("fs", "tp"), axis=0, tiled=False)
    tail = share[size // nfs :]
    last = jnp.concatenate(
        [tail[:, index * narrow : (index + 1) * narrow] for index in range(fold)], axis=0
    )
    blocks, last = lax.optimization_barrier((blocks, last))
    gathered = lax.all_gather(last, ("fs", "rep", "tp"), axis=0, tiled=False)
    mine = polynomial(blocks, ntp)
    columns = lax.all_gather(mine, "rep", axis=0, tiled=False)
    factors = [columns[index] for index in range(nrep)]
    factors.append(polynomial(gathered, ntp))

    results = []
    for moment, weight, whole, factor in zip(moments, weights, wholes, factors):
        rows = moment.shape[0] * nfs * nrep
        final = jnp.dot(whole, factor, preferred_element_type=jnp.float32)
        results.append(moment)
        results.append(SHRINK * weight - RATE * math.sqrt(rows) * final)
    return tuple(results)


def solution(mesh):
    sizes = mesh.shape
    split = P(("fs", "rep"), "tp")
    return jax.shard_map(
        functools.partial(local, sizes["fs"], sizes["tp"], sizes["rep"]),
        mesh=mesh,
        in_specs=(P("rep", "fs", "tp"), split, split) * 3,
        out_specs=(split,) * 6,
        check_vma=False,
    )
```

time: 570 us -> 464 us (0.81)
  other arithmetic: 48.8 us -> 16.7 us
  waiting for transfers between devices: 287 us -> 260 us
  Pallas kernels: 155 us -> 130 us
  local copies, waits for them, and re-layouts: 28.4 us -> 4.32 us
    pallas_call x2, Pallas kernels: 155 us -> 130 us  [polynomial(): pl.pallas_call(functools.partial(polynomial_kernel, across, tile), out_sh...]
    all_gather x2, waiting for transfers between devices: 81.8 us -> 64.6 us  [local(): lax.all_gather(start, 'tp', axis=1, tiled=True)]
    convert_element_type x2 -> x0, other arithmetic: 13.4 us -> none  [normalized(): wide = raw.astype(jnp.float32)]
    reduce_scatter x2 -> x1, waiting for transfers between devices: 67.4 us -> 55 us  [local(): lax.psum_scatter(both.reshape(-1, width), ('fs', 'rep'), scatter_dimensio...]
    convert_element_type x1 -> x0, local copies, waits for them, and re-layouts: 12.2 us -> none  [normalized(): return ((wide / ratio).astype(jnp.bfloat16), lax.rsqrt(ratio))]
    reduce_sum x2 -> x0, other arithmetic: 11.5 us -> none  [normalized(): first = jnp.sum(jnp.where(here == there, wide, 0.0))]
    unnamed x28 -> x24, local copies, waits for them, and re-layouts: 11.6 us -> 1.63 us
    another operation x2 -> x0, other arithmetic: 8.7 us -> none
  transfers between devices with their start and end apart: 10 -> 9, of which waited for: 8 -> 7; matrix products, arithmetic and copies ran while one was open for 15% -> 4% of each run, Pallas kernels for 27% -> 28%
where the time goes in v2:
time: 464 us; the launch traced here: 463 us
  waiting for transfers between devices  260 us (56%)
  Pallas kernels  130 us (28%)
  blocking collectives  19.3 us (4%)
  matrix products  18.7 us (4%)
  other arithmetic  16.7 us (4%)
  between operations  14 us (3%)
    pallas_call x2, Pallas kernels, polynomial(): pl.pallas_call(functools.partial(polynomial_kernel, across, tile), out_sh...  130 us
    all_gather x1, waiting for transfers between devices, local(): lax.all_gather(share[:size // nfs], ('fs', 'tp'), axis=0, tiled=False)  111 us
    all_gather x2, waiting for transfers between devices, local(): lax.all_gather(start, 'tp', axis=1, tiled=True)  64.6 us
    reduce_scatter x1, waiting for transfers between devices, local(): lax.psum_scatter(both.reshape(-1, width), ('fs', 'rep'), scatter_dimensio...  55 us
    reduce_scatter x3, waiting for transfers between devices, local(): lax.psum_scatter(g.astype(jnp.bfloat16), 'rep', scatter_dimension=1, tile...  29 us
    all_gather x1, blocking collectives, local(): lax.all_gather(start, 'tp', axis=1, tiled=True)  19.3 us
    dot_general x3, matrix products, local(): final = jnp.dot(whole, factor, preferred_element_type=jnp.float32)  9.57 us
  transfers between devices with their start and end apart: 9, of which 7 were waited for; matrix products, arithmetic and copies ran while one was open for 4% of the time, Pallas kernels for 28%

profile of v2, /device:TPU:0, one launch (start us, length us, event | category | flops | bytes accessed | tf_op | source)
XLA Modules:
  0.0 463.2 jit_solution(13336927461155373531)
XLA Ops:
  7.2 1.8 convert_element_type.53
  9.0 0.0 reduce-scatter.7.cloned.1.call-start
  9.1 3.2 convert_element_type.49
  12.4 1.3 convert_element_type.45
  13.8 7.5 %reduce-scatter.9.cloned.1.call-done = bf16[1,256,256]{2,1,0:T(8,128)(2,1)} async-done(((bf16[1,512,256]{2,1,0:T(8,128)(2,1)}), bf16[1,256,256]{2,1,0:T(8,128)(2,1)}) %reduce-scatter.9.cloned.1.call-update) | async-done | bytes 131088 | tf_op jit(solution)/shard_map/reduce_scatter | solution.py:143
  21.3 1.6 fusion.15
  22.9 11.2 %reduce-scatter.7.cloned.1.call-done = bf16[1,704,512]{2,1,0:T(8,128)(2,1)} async-done(((bf16[1,1408,512]{2,1,0:T(8,128)(2,1)}), bf16[1,704,512]{2,1,0:T(8,128)(2,1)}) %reduce-scatter.7.cloned.1.call-update) | async-done | bytes 720912 | tf_op jit(solution)/shard_map/reduce_scatter | solution.py:143
  34.1 2.7 fusion.16
  36.8 10.3 %reduce-scatter.5.cloned.1.call-done = bf16[1,704,512]{2,1,0:T(8,128)(2,1)} async-done(((bf16[1,1408,512]{2,1,0:T(8,128)(2,1)}), bf16[1,704,512]{2,1,0:T(8,128)(2,1)}) %reduce-scatter.5.cloned.1.call-update) | async-done | bytes 720912 | tf_op jit(solution)/shard_map/reduce_scatter | solution.py:143
  47.1 2.7 fusion.17
  49.9 0.5 all-gather.9.cloned.1.call-update
  50.5 19.3 %all_gather.29 = bf16[256,1024]{1,0:T(8,128)(2,1)S(1)} all-gather(bf16[256,256]{1,0:T(8,128)(2,1)S(1)} %get-tuple-element.13), channel_id=1, replica_groups=mesh['fs'=4,'tp'=4,'rep'=2] {'tp'}, dimensions={1}, use_global_device_ids=true | all-gather | bytes 655360 | tf_op jit(solution)/shard_map/all_gather | solution.py:149
  69.8 0.4 convolution_convert_fusion.2
  70.2 25.8 %all-gather.11.cloned.1.call-done = bf16[704,2048]{1,0:T(8,128)(2,1)} async-done(((bf16[704,512]{1,0:T(8,128)(2,1)}), bf16[704,2048]{1,0:T(8,128)(2,1)}) %all-gather.11.cloned.1.call-update) | async-done | bytes 2883600 | tf_op jit(solution)/shard_map/all_gather | solution.py:149
  96.0 5.0 %convolution_convert_fusion = bf16[2048,512]{1,0:T(8,128)(2,1)} fusion(bf16[704,2048]{1,0:T(8,128)(2,1)} %all-gather.11.cloned.1.call-done, bf16[704,512]{1,0:T(8,128)(2,1)S(1)} %copy-done.2), kind=kOutput, calls=%fused_computation.2 | convolution fusion | flops 1477443584 | bytes 5701632 | tf_op jit(solution)/shard_map/dot_general | solution.py:135
  101.0 38.8 %all-gather.9.cloned.1.call-done = bf16[704,2048]{1,0:T(8,128)(2,1)} async-done(((bf16[704,512]{1,0:T(8,128)(2,1)}), bf16[704,2048]{1,0:T(8,128)(2,1)}) %all-gather.9.cloned.1.call-update) | async-done | bytes 2883600 | tf_op jit(solution)/shard_map/all_gather | solution.py:149
  139.8 3.8 convolution_convert_fusion.1
  143.6 0.4 pad_maximum_fusion
  144.0 2.3 maximum_maximum_fusion
  146.3 0.0 all-gather.13.cloned.1.call-start
  146.4 55.0 %reduce-scatter.11.cloned.1.call-done = bf16[576,512]{1,0:T(8,128)(2,1)} async-done(((bf16[4608,512]{1,0:T(8,128)(2,1)}), bf16[576,512]{1,0:T(8,128)(2,1)}) %reduce-scatter.11.cloned.1.call-update) | async-done | bytes 589840 | tf_op jit(solution)/shard_map/reduce_scatter | solution.py:161
  201.4 1.9 slice.35
  203.3 0.8 fusion.18
  204.1 0.6 pad_maximum_fusion.1
  204.7 110.8 %all-gather.13.cloned.1.call-done = bf16[8192,512]{1,0:T(8,128)(2,1)} async-done(((bf16[512,512]{1,0:T(8,128)(2,1)}), bf16[8192,512]{1,0:T(8,128)(2,1)}) %all-gather.13.cloned.1.call-update) | async-done | bytes 8388624 | tf_op jit(solution)/shard_map/all_gather | solution.py:164
  315.5 0.2 all-gather.15.cloned.1.call-start
  315.8 110.2 %polynomial_2048.1 = bf16[2048,512]{1,0:T(8,128)(2,1)} custom-call(s32[1,1]{1,0:T(1,128)} %bitcast.3.column_ref, bf16[16,512,512]{2,1,0:T(8,128)(2,1)} %bitcast.48), custom_call_target="tpu_custom_call" | custom-call | flops 85899345920 | bytes 12582912 | tf_op jit(solution)/shard_map/polynomial_2048/pallas_call | solution.py:115
  426.0 1.6 copy-done
  427.6 19.5 %polynomial_1024.1 = bf16[1024,256]{1,0:T(8,128)(2,1)S(1)} custom-call(s32[1,1]{1,0:T(1,128)} %bitcast.3.column_ref, bf16[32,128,256]{2,1,0:T(8,128)(2,1)S(1)} %bitcast.42), custom_call_target="tpu_custom_call" | custom-call | flops 10737418240 | bytes 3145728 | tf_op jit(solution)/shard_map/polynomial_1024/pallas_call | solution.py:115
  447.1 1.0 fusion.14
  448.1 5.8 %multiply_subtract_fusion.1 = f32[704,512]{1,0:T(8,128)} fusion(f32[704,512]{1,0:T(8,128)} %param.11, bf16[704,2048]{1,0:T(8,128)(2,1)} %all-gather.9.cloned.1.call-done, bf16[4096,512]{1,0:T(8,128)(2,1)} %all-gather.15.cloned.1.call-done), kind=kOutput, calls=%fused_computation.13 | convolution fusion | flops 1477476352 | bytes 7864320 | tf_op jit(solution)/shard_map/dot_general | solution.py:179
  453.9 2.8 multiply_subtract_fusion
  (40 shorter events, 0.5 us)
Async XLA Ops:
  7.2 14.1 %reduce-scatter.9.cloned.1.call-start = ((), (), s32[]{:S(2)}) async-start(), calls=%async_computation.6 | async-start | bytes 393216 | tf_op jit(solution)/shard_map/reduce_scatter | solution.py:143
  9.0 3.4 copy-start.1
  9.0 25.1 %reduce-scatter.7.cloned.1.call-start = ((), (), s32[]{:S(2)}) async-start(), calls=%async_computation.5 | async-start | bytes 2162688 | tf_op jit(solution)/shard_map/reduce_scatter | solution.py:143
  12.3 8.9 %copy-start.7 = (f32[256,256]{1,0:T(8,128)S(1)}, f32[256,256]{1,0:T(8,128)}, u32[]{:S(2)}) copy-start(f32[256,256]{1,0:T(8,128)} %param.16) | copy-start | bytes 786436
  12.4 34.7 %reduce-scatter.5.cloned.1.call-start = ((), (), s32[]{:S(2)}) async-start(), calls=%async_computation.4 | async-start | bytes 2162688 | tf_op jit(solution)/shard_map/reduce_scatter | solution.py:143
  13.7 20.4 %copy-start.5 = (f32[704,512]{1,0:T(8,128)S(1)}, f32[704,512]{1,0:T(8,128)}, u32[]{:S(2)}) copy-start(f32[704,512]{1,0:T(8,128)} %param.13) | copy-start | bytes 4325380
  13.7 82.2 %all-gather.11.cloned.1.call-start = ((), (), s32[]{:S(2)}) async-start(), calls=%async_computation.8 | async-start | bytes 3604480 | tf_op jit(solution)/shard_map/all_gather | solution.py:149
  22.9 24.2 %copy-start.6 = (f32[704,512]{1,0:T(8,128)S(1)}, f32[704,512]{1,0:T(8,128)}, u32[]{:S(2)}) copy-start(f32[704,512]{1,0:T(8,128)} %param.10) | copy-start | bytes 4325380
  49.8 46.1 %copy-start.2 = (bf16[704,512]{1,0:T(8,128)(2,1)S(1)}, bf16[704,512]{1,0:T(8,128)(2,1)}, u32[]{:S(2)}) copy-start(bf16[704,512]{1,0:T(8,128)(2,1)} %get-tuple-element.12) | copy-start | bytes 2162692
  49.8 89.9 %all-gather.9.cloned.1.call-start = ((), (), s32[]{:S(2)}) async-start(), calls=%async_computation.7 | async-start | bytes 3604480 | tf_op jit(solution)/shard_map/all_gather | solution.py:149
  50.4 150.9 %reduce-scatter.11.cloned.1.call-start = ((), (), s32[]{:S(2)}) async-start(), calls=%async_computation.9 | async-start | bytes 5308416 | tf_op jit(solution)/shard_map/reduce_scatter | solution.py:161
  70.2 69.6 %copy-start.3 = (bf16[704,512]{1,0:T(8,128)(2,1)S(1)}, bf16[704,512]{1,0:T(8,128)(2,1)}, u32[]{:S(2)}) copy-start(bf16[704,512]{1,0:T(8,128)(2,1)} %get-tuple-element.11) | copy-start | bytes 2162692
  139.8 3.8 copy-start.4
  146.3 169.2 %all-gather.13.cloned.1.call-start = ((), (), s32[]{:S(2)}) async-start(), calls=%async_computation.10 | async-start | bytes 8912896 | tf_op jit(solution)/shard_map/all_gather | solution.py:164
  203.3 222.7 %all-gather.17.cloned.1.call-start = ((), (), s32[]{:S(2)}) async-start(), calls=%async_computation.12 | async-start | bytes 2162688 | tf_op jit(solution)/shard_map/all_gather | solution.py:170
  315.5 132.6 %all-gather.15.cloned.1.call-start = ((), (), s32[]{:S(2)}) async-start(), calls=%async_computation.11 | async-start | bytes 6291456 | tf_op jit(solution)/shard_map/all_gather | solution.py:172
  426.0 1.6 copy-start
  427.6 19.5 %copy-start.8 = (f32[256,256]{1,0:T(8,128)S(1)}, f32[256,256]{1,0:T(8,128)}, u32[]{:S(2)}) copy-start(f32[256,256]{1,0:T(8,128)} %param.17) | copy-start | bytes 786436
  448.1 5.8 %copy-start.10 = (bf16[704,2048]{1,0:T(8,128)(2,1)S(1)}, bf16[704,2048]{1,0:T(8,128)(2,1)}, u32[]{:S(2)}) copy-start(bf16[704,2048]{1,0:T(8,128)(2,1)} %all-gather.11.cloned.1.call-done) | copy-start | bytes 8650756
  448.1 5.8 %copy-start.9 = (bf16[4096,512]{1,0:T(8,128)(2,1)S(1)}, bf16[4096,512]{1,0:T(8,128)(2,1)}, u32[]{:S(2)}) copy-start(bf16[4096,512]{1,0:T(8,128)(2,1)} %all-gather.15.cloned.1.call-done) | copy-start | bytes 12582916
  448.1 5.8 %copy-start.11 = (f32[704,512]{1,0:T(8,128)S(1)}, f32[704,512]{1,0:T(8,128)}, u32[]{:S(2)}) copy-start(f32[704,512]{1,0:T(8,128)} %param.14) | copy-start | bytes 4325380
Sparse Core Ops, SparseCore 0:
  10.8 10.4 reduce-scatter.8
  24.1 9.9 reduce-scatter.6
  36.9 10.1 reduce-scatter.4
  50.0 45.9 all-gather.10
  98.2 41.5 all-gather.8
  146.5 54.8 reduce-scatter.10
  204.7 110.7 all-gather.12
  319.0 54.4 all-gather.16
  426.1 11.8 all-gather.14
